TPU v7x, 32 devices: a whole 2x2x4 slice. The times are simulated.
32 devices in a mesh: sp: 8 (over z, y), tp: 4 (over x, core).
Axes of the slice: x: 2, y: 2, z: 4, core: 2. Of those that a mesh axis runs over, the one named last changes fastest.
Arguments:
- stream_in: bfloat16 [6144, 2048], P(('sp', 'tp')), may hold values from -6 to 6
- query_wide: bfloat16 [6144, 512], P('sp', 'tp'), may hold values from -6 to 6
- key_wide: bfloat16 [6144, 512], P('sp', 'tp'), may hold values from -6 to 6
- value_wide: bfloat16 [6144, 512], P('sp', 'tp'), may hold values from -6 to 6
- gate_wide: bfloat16 [6144, 512], P('sp', 'tp'), may hold values from -6 to 6
- decay_wide: float32 [4, 6144], P('tp', 'sp'), may hold values from -2.3 to 0, as said below
- query_narrow: bfloat16 [6144, 512], P('sp', 'tp'), may hold values from -6 to 6
- key_narrow: bfloat16 [6144, 512], P('sp', 'tp'), may hold values from -6 to 6
- value_narrow: bfloat16 [6144, 512], P('sp', 'tp'), may hold values from -6 to 6
- gate_narrow: bfloat16 [6144, 512], P('sp', 'tp'), may hold values from -6 to 6
- decay_narrow: float32 [8, 6144], P('tp', 'sp'), may hold values from -2.3 to 0, as said below
- output_wide: bfloat16 [512, 2048], P('tp'), may hold values from -0.25 to 0.25
- output_narrow: bfloat16 [512, 2048], P('tp'), may hold values from -0.25 to 0.25
- norm_gain: bfloat16 [2048], replicated, may hold values from 0.099609375 to 1.8984375
- up_weight: bfloat16 [2048, 8192], P('sp', 'tp'), may hold values from -0.125 to 0.125
- down_weight: bfloat16 [8192, 2048], P('tp', 'sp'), may hold values from -0.0625 to 0.0625
Outputs:
- layer_out: bfloat16 [6144, 2048], P(('sp', 'tp'))
Inputs may be any that keep to these rules, and one draw needn't show every extreme that they name: `decay_wide`: each entry is the logarithm of one head's retention factor at one position. `decay_narrow`: each entry is the logarithm of one head's retention factor at one position.
All inputs are finite; a program needn't handle non-finite values.
Results may differ from a plain program's by a relative error of at most 0.02.
Values may be sent and summed in bfloat16 or wider, within the bound.
A program may use at most 128 MiB of HBM per device.

v0:
```python
import jax
import jax.numpy as jnp
from jax import lax
from jax.sharding import PartitionSpec as P

HDW = 128
HDN = 64
BLOCK = 128


head_eps = 1e-05
norm_eps = 1e-06
rope_base = 10000.0


def carried_in(shard, axis, join, neutral):
    place = lax.axis_index(axis)
    gathered = jax.tree.map(
        lambda a, kind: lax.all_gather(a.astype(kind), axis),
        shard,
        (jnp.bfloat16, jnp.bfloat16, jnp.bfloat16, jnp.bfloat16),
    )
    state = jax.tree.map(lambda a, e: jnp.zeros_like(a) + jnp.asarray(e, a.dtype), shard, neutral)

    def one(turn, state):
        return join(
            state,
            jax.tree.map(
                lambda a, own: lax.dynamic_index_in_dim(a, turn, 0, False).astype(own.dtype),
                gathered,
                shard,
            ),
        )

    return lax.fori_loop(0, place, one, state)


def rotate(values, places):
    half = values.shape[-1] // 2
    inverse = rope_base ** (-jnp.arange(half, dtype=jnp.float32) / half)
    angles = places[:, None] * inverse[None, :]
    cosine = jnp.cos(angles)[:, None, :]
    sine = jnp.sin(angles)[:, None, :]
    front = values[..., :half]
    back = values[..., half:]
    return jnp.concatenate([front * cosine - back * sine, back * cosine + front * sine], axis=-1)


def block_step(carried, inputs):
    query, keys, values, log_rate = inputs
    running = jnp.cumsum(log_rate, axis=0)
    spread = running[:, None, :] - running[None, :, :]
    length = log_rate.shape[0]
    lower = (jnp.arange(length)[:, None] >= jnp.arange(length)[None, :])[:, :, None]
    factor = jnp.where(lower, jnp.exp(jnp.minimum(spread, 0.0)), 0.0)
    scores = jnp.einsum("thd,shd->tsh", query, keys) * factor
    within = jnp.einsum("tsh,she->the", scores, values)
    across = jnp.einsum("thd,hde->the", query, carried) * jnp.exp(running)[:, :, None]
    tail_decay = jnp.exp(running[-1][None, :] - running)
    updated = jnp.exp(running[-1])[:, None, None] * carried + jnp.einsum(
        "shd,she->hde", keys * tail_decay[:, :, None], values
    )
    return (updated, within + across)


def head_norm(values):
    centre = values - jnp.mean(values, axis=-1, keepdims=True)
    spread = jnp.mean(centre * centre, axis=-1, keepdims=True)
    return centre * lax.rsqrt(spread + head_eps)


def local_group(query, keys, values, log_rate, width, places):
    length = query.shape[0]
    count_of_heads = query.shape[1] // width
    blocks = length // BLOCK

    def split(array):
        return array.astype(jnp.float32).reshape(length, count_of_heads, width)

    query_rot = rotate(split(query), places)
    keys_rot = rotate(split(keys), places) * width ** (-0.5)
    rates = log_rate.T
    carried = jnp.zeros((count_of_heads, width, width), jnp.float32)
    final_state, outputs = lax.scan(
        block_step,
        carried,
        (
            query_rot.reshape(blocks, BLOCK, count_of_heads, width),
            keys_rot.reshape(blocks, BLOCK, count_of_heads, width),
            split(values).reshape(blocks, BLOCK, count_of_heads, width),
            rates.reshape(blocks, BLOCK, count_of_heads),
        ),
    )
    running = jnp.cumsum(rates, axis=0)
    return (
        query_rot,
        outputs.reshape(length, count_of_heads, width),
        final_state,
        jnp.exp(running[-1]),
        running,
    )


def finish_group(query_rot, outputs, incoming, running, gate):
    length = outputs.shape[0]
    outputs = (
        outputs + jnp.einsum("thd,hde->the", query_rot, incoming) * jnp.exp(running)[:, :, None]
    )
    normed = head_norm(outputs).reshape(length, -1)
    return (jax.nn.silu(gate.astype(jnp.float32)) * normed).astype(jnp.bfloat16)


def chain(earlier, later):
    rate_wide, memory_wide, rate_narrow, memory_narrow = earlier
    later_rate_wide, later_memory_wide, later_rate_narrow, later_memory_narrow = later
    return (
        rate_wide * later_rate_wide,
        memory_wide * later_rate_wide[:, None, None] + later_memory_wide,
        rate_narrow * later_rate_narrow,
        memory_narrow * later_rate_narrow[:, None, None] + later_memory_narrow,
    )


def row_norm(middle, norm_gain):
    middle_f = middle.astype(jnp.float32)
    scale = lax.rsqrt(jnp.mean(middle_f * middle_f, axis=-1, keepdims=True) + norm_eps)
    return (middle_f * scale * norm_gain.astype(jnp.float32)).astype(jnp.bfloat16)


def on_device(
    stream_in,
    query_wide,
    key_wide,
    value_wide,
    gate_wide,
    decay_wide,
    query_narrow,
    key_narrow,
    value_narrow,
    gate_narrow,
    decay_narrow,
    output_wide,
    output_narrow,
    norm_gain,
    up_weight,
    down_weight,
):
    length = query_wide.shape[0]
    places = (lax.axis_index("sp") * length + jnp.arange(length, dtype=jnp.int32)).astype(
        jnp.float32
    )
    wide_query, wide_out, wide_state, wide_total, wide_running = local_group(
        query_wide, key_wide, value_wide, decay_wide, HDW, places
    )
    narrow_query, narrow_out, narrow_state, narrow_total, narrow_running = local_group(
        query_narrow, key_narrow, value_narrow, decay_narrow, HDN, places
    )
    identity = (
        jnp.ones_like(wide_total),
        jnp.zeros_like(wide_state),
        jnp.ones_like(narrow_total),
        jnp.zeros_like(narrow_state),
    )
    incoming = carried_in(
        (wide_total, wide_state, narrow_total, narrow_state), "sp", chain, identity
    )
    mixed_wide = finish_group(wide_query, wide_out, incoming[1], wide_running, gate_wide)
    mixed_narrow = finish_group(narrow_query, narrow_out, incoming[3], narrow_running, gate_narrow)
    mixed_sum = lax.psum_scatter(
        (
            jnp.dot(mixed_wide, output_wide, preferred_element_type=jnp.float32)
            + jnp.dot(mixed_narrow, output_narrow, preferred_element_type=jnp.float32)
        ).astype(jnp.bfloat16),
        "tp",
        scatter_dimension=0,
        tiled=True,
    ).astype(jnp.float32)
    middle = (stream_in.astype(jnp.float32) + mixed_sum).astype(jnp.bfloat16)
    normed = lax.all_gather(row_norm(middle, norm_gain), "tp", axis=0, tiled=True)
    up_sum = jnp.dot(
        normed,
        lax.all_gather(up_weight, "sp", axis=0, tiled=True),
        preferred_element_type=jnp.float32,
    )
    hidden = jnp.square(jax.nn.relu(up_sum)).astype(jnp.bfloat16)
    down_sum = jnp.dot(
        hidden,
        lax.all_gather(down_weight, "sp", axis=1, tiled=True),
        preferred_element_type=jnp.float32,
    )
    down_rows = lax.psum_scatter(
        down_sum.astype(jnp.bfloat16), "tp", scatter_dimension=0, tiled=True
    ).astype(jnp.float32)
    return (middle.astype(jnp.float32) + down_rows).astype(jnp.bfloat16)


def solution(mesh):
    in_specs = (
        P(("sp", "tp"), None),
        P("sp", "tp"),
        P("sp", "tp"),
        P("sp", "tp"),
        P("sp", "tp"),
        P("tp", "sp"),
        P("sp", "tp"),
        P("sp", "tp"),
        P("sp", "tp"),
        P("sp", "tp"),
        P("tp", "sp"),
        P("tp", None),
        P("tp", None),
        P(),
        P("sp", "tp"),
        P("tp", "sp"),
    )
    out_specs = P(("sp", "tp"), None)
    return jax.shard_map(
        on_device, mesh=mesh, in_specs=in_specs, out_specs=out_specs, check_vma=False
    )
```

profile of v0, /device:TPU:17, one launch (start us, length us, event | category | flops | bytes accessed | tf_op | source)
XLA Modules:
  0.0 576.9 jit_solution(15378131517314459082)
XLA Ops:
  11.9 25.0 %while.43 = (s32[]{:T(128)}, f32[2,64,64]{2,1,0:T(8,128)S(1)}, f32[6,128,2,64]{1,0,3,2:T(8,128)}, f32[6,128,2]{2,1,0:T(8,128)S(1)}, f32[6,128,2,64]{1,0,3,2:T(8,...) while((s32[]{:T(128)}, f32[2,64,64]{2,1,0:T(8,128)S(1)}, ...), condition=%wide.region_9.10_spmd.clone, body=%wide.region_7.9_spmd.clone.sunk | while | flops 12877827 | bytes 1099440 | solution.py:84
  13.0 2.8 dynamic_update_slice.14
  17.2 2.8 dynamic_update_slice.14
  21.4 2.8 dynamic_update_slice.14
  25.5 2.8 dynamic_update_slice.14
  29.7 2.8 dynamic_update_slice.14
  33.8 2.8 dynamic_update_slice.14
  36.9 22.3 %all-gather.1 = bf16[16,64,64]{2,1,0:T(8,128)(2,1)} all-gather(bf16[2,64,64]{2,1,0:T(8,128)(2,1)S(1)} %convert_element_type.115), channel_id=3, replica_groups=mesh['sp'=8,'tp'=4] {'sp'}, dimensions={0}, use_global_device_ids=true | all-gather | bytes 147456 | tf_op jit(solution)/shard_map/all_gather | solution.py:19
  61.2 1.9 fusion.74
  64.2 27.8 %while.42 = (s32[]{:T(128)}, f32[1,128,128]{2,1,0:T(8,128)S(1)}, f32[6,128,1,128]{3,1,0,2:T(8,128)}, f32[6,128,1]{1,2,0:T(1,128)}, f32[6,128,1,128]{3,2,1,0:T(1,...) while((s32[]{:T(128)}, f32[1,128,128]{2,1,0:T(8,128)S(1)}, ...), condition=%wide.region_2.3_spmd.clone, body=%wide.region_0.2_spmd.clone.sunk | while | flops 17006596 | bytes 1515172 | solution.py:84
  92.0 24.6 %all-gather = bf16[8,128,128]{2,1,0:T(8,128)(2,1)S(1)} all-gather(bf16[1,128,128]{2,1,0:T(8,128)(2,1)S(1)} %convert_element_type.113), channel_id=2, replica_groups=mesh['sp'=8,'tp'=4] {'sp'}, dimensions={0}, use_global_device_ids=true | all-gather | bytes 294912 | tf_op jit(solution)/shard_map/all_gather | solution.py:19
  120.5 16.7 %all-reduce = bf16[8]{0:T(256)(128)(2,1)S(1)} all-reduce(bf16[8]{0:T(256)(128)(2,1)S(1)} %dynamic-update-slice), channel_id=1, replica_groups=mesh['sp'=8,'tp'=4] {'sp'}, use_global_device_ids=true, to_apply=%add | all-reduce | flops 8 | bytes 32
  138.3 13.2 %all-gather.2 = bf16[8,1,2]{2,1,0:T(2,128)(2,1)S(1)} all-gather(bf16[1,1,2]{2,1,0:T(2,128)(2,1)S(1)} %bitcast.321), channel_id=1, replica_groups=mesh['sp'=8,'tp'=4] {'sp'}, dimensions={0}, use_global_device_ids=true | all-gather | bytes 36 | tf_op jit(solution)/shard_map/all_gather | solution.py:19
  151.6 9.4 %while.41 = (s32[]{:T(128)}, f32[1,128,128]{2,1,0:T(8,128)S(1)}, f32[2,64,64]{2,1,0:T(8,128)S(1)}, s32[]{:T(128)}, bf16[8,1]{0,1:T(2,128)(2,1)S(1)}, /*index=5*/...) while((s32[]{:T(128)}, f32[1,128,128]{2,1,0:T(8,128)S(1)}, ...), condition=%wide.region_11.12_spmd, body=%wide.region_10.11_spmd.sunk | while | flops 73736 | bytes 245969 | solution.py:35
  164.7 2.7 add_convert_fusion
  168.1 67.6 %reduce-scatter.3.cloned.1.call-done = bf16[192,2048]{1,0:T(8,128)(2,1)} async-done(((bf16[768,2048]{1,0:T(8,128)(2,1)}), bf16[192,2048]{1,0:T(8,128)(2,1)}) %reduce-scatter.3.cloned.1.call-update) | async-done | bytes 786448 | tf_op jit(solution)/shard_map/reduce_scatter | solution.py:169
  237.2 2.3 fusion.49
  241.1 27.7 %all-gather.7.cloned.1.call-done = bf16[768,2048]{1,0:T(8,128)(2,1)} async-done(((bf16[192,2048]{1,0:T(8,128)(2,1)}), bf16[768,2048]{1,0:T(8,128)(2,1)}) %all-gather.7.cloned.1.call-update) | async-done | bytes 3145744 | tf_op jit(solution)/shard_map/all_gather | solution.py:179
  268.8 124.6 %all-gather.9.cloned.1.call-done = bf16[2048,2048]{1,0:T(8,128)(2,1)} async-done(((bf16[256,2048]{1,0:T(8,128)(2,1)}), bf16[2048,2048]{1,0:T(8,128)(2,1)}) %all-gather.9.cloned.1.call-update) | async-done | bytes 8388624 | tf_op jit(solution)/shard_map/all_gather | solution.py:182
  393.4 11.9 %multiply_convert_fusion = bf16[768,2048]{1,0:T(8,128)(2,1)} fusion(bf16[768,2048]{1,0:T(8,128)(2,1)} %all-gather.7.cloned.1.call-done, bf16[2048,2048]{1,0:T(8,128)(2,1)} %all-gather.9.cloned.1.call-done), kind=kOutput, calls=%fused_computation.73 | convolution fusion | flops 6447169536 | bytes 14680064 | tf_op jit(solution)/shard_map/dot_general | solution.py:180
  405.2 113.2 %all-gather.11.cloned.1.call-done = bf16[2048,2048]{1,0:T(8,128)(2,1)} async-done(((bf16[2048,256]{1,0:T(8,128)(2,1)}), bf16[2048,2048]{1,0:T(8,128)(2,1)}) %all-gather.11.cloned.1.call-update) | async-done | bytes 8388624 | tf_op jit(solution)/shard_map/all_gather | solution.py:188
  518.4 11.9 %convolution_convert_fusion = bf16[768,2048]{1,0:T(8,128)(2,1)} fusion(bf16[768,2048]{1,0:T(8,128)(2,1)} %multiply_convert_fusion, bf16[2048,2048]{1,0:T(8,128)(2,1)} %all-gather.11.cloned.1.call-done), kind=kOutput, calls=%fused_computation.75 | convolution fusion | flops 6444023808 | bytes 14680064 | tf_op jit(solution)/shard_map/dot_general | solution.py:186
  530.3 37.7 %reduce-scatter.5.cloned.1.call-done = bf16[192,2048]{1,0:T(8,128)(2,1)} async-done(((bf16[768,2048]{1,0:T(8,128)(2,1)}), bf16[192,2048]{1,0:T(8,128)(2,1)}) %reduce-scatter.5.cloned.1.call-update) | async-done | bytes 786448 | tf_op jit(solution)/shard_map/reduce_scatter | solution.py:191
  568.0 2.4 fusion.50
  (281 shorter events, 57.2 us)
Async XLA Ops:
  6.5 157.1 %copy-start = (bf16[128,2048]{1,0:T(8,128)(2,1)S(1)}, bf16[128,2048]{1,0:T(8,128)(2,1)}, u32[]{:S(2)}) copy-start(bf16[128,2048]{1,0:T(8,128)(2,1)} %param.33) | copy-start | bytes 1572868
  6.5 4.5 copy-start.8
  6.5 229.2 %reduce-scatter.3.cloned.1.call-start = ((), (), s32[]{:S(2)}) async-start(), calls=%async_computation.2 | async-start | bytes 3932160 | tf_op jit(solution)/shard_map/reduce_scatter | solution.py:169
  9.3 2.3 copy-start.9
  11.9 48.3 %copy-start.5 = (bf16[768,128]{1,0:T(8,128)(2,1)S(1)}, bf16[768,128]{1,0:T(8,128)(2,1)}, u32[]{:S(2)}) copy-start(bf16[768,128]{1,0:T(8,128)(2,1)} %param.23) | copy-start | bytes 589828
  64.1 54.9 %copy-start.11 = (u32[32]{0:T(128)S(1)}, u32[32]{0:T(128)}, u32[]{:S(2)}) copy-start(u32[32]{0:T(128)} %constant.123) | copy-start | bytes 388
  91.9 70.7 %copy-start.6 = (bf16[768,128]{1,0:T(8,128)(2,1)S(1)}, bf16[768,128]{1,0:T(8,128)(2,1)}, u32[]{:S(2)}) copy-start(bf16[768,128]{1,0:T(8,128)(2,1)} %param.31) | copy-start | bytes 589828
  91.9 70.8 %copy-start.4 = (f32[6,128,1,128]{3,1,0,2:T(8,128)S(1)}, f32[6,128,1,128]{3,1,0,2:T(8,128)}, u32[]{:S(2)}) copy-start(f32[6,128,1,128]{3,1,0,2:T(8,128)} %get-tuple-element.151) | copy-start | bytes 1179652
  161.0 2.4 copy-start.7
  163.7 1.0 copy-start.3
  167.4 0.7 copy-start.10
  167.4 68.3 %copy-start.1 = (bf16[192,2048]{1,0:T(8,128)(2,1)S(1)}, bf16[192,2048]{1,0:T(8,128)(2,1)}, u32[]{:S(2)}) copy-start(bf16[192,2048]{1,0:T(8,128)(2,1)} %param.22) | copy-start | bytes 2359300
  167.4 101.3 %all-gather.7.cloned.1.call-start = ((), (), s32[]{:S(2)}) async-start(), calls=%async_computation.3 | async-start | bytes 3932160 | tf_op jit(solution)/shard_map/all_gather | solution.py:179
  239.5 153.9 %all-gather.9.cloned.1.call-start = ((), (), s32[]{:S(2)}) async-start(), calls=%async_computation.4 | async-start | bytes 9437184 | tf_op jit(solution)/shard_map/all_gather | solution.py:182
  240.3 278.2 %all-gather.11.cloned.1.call-start = ((), (), s32[]{:S(2)}) async-start(), calls=%async_computation.5 | async-start | bytes 9437184 | tf_op jit(solution)/shard_map/all_gather | solution.py:188
  240.8 327.1 %reduce-scatter.5.cloned.1.call-start = ((), (), s32[]{:S(2)}) async-start(), calls=%async_computation.6 | async-start | bytes 3932160 | tf_op jit(solution)/shard_map/reduce_scatter | solution.py:191
  530.3 37.7 %copy-start.2 = (bf16[192,2048]{1,0:T(8,128)(2,1)S(1)}, bf16[192,2048]{1,0:T(8,128)(2,1)}, u32[]{:S(2)}) copy-start(bf16[192,2048]{1,0:T(8,128)(2,1)} %reduce-scatter.3.cloned.1.call-done) | copy-start | bytes 2359300
Sparse Core Ops, SparseCore 0:
  167.6 68.1 reduce-scatter.2
  239.7 29.0 all-gather.6
  270.9 122.4 all-gather.8
  395.3 123.1 all-gather.10
  530.4 37.5 reduce-scatter.4
where the time goes:
time: 580 us; the launch traced here: 577 us
  waiting for transfers between devices  372 us (64%)
  blocking collectives  76.8 us (13%)
  local copies, waits for them, and re-layouts  42.9 us (7%)
  matrix products  36.5 us (6%)
  other arithmetic  25.9 us (4%)
  between operations  14.9 us (3%)
  loops' own time  7.6 us (1%)
    all_gather x1, waiting for transfers between devices, on_device(): lax.all_gather(up_weight, 'sp', axis=0, tiled=True)  125 us
    all_gather x1, waiting for transfers between devices, on_device(): lax.all_gather(down_weight, 'sp', axis=1, tiled=True)  113 us
    reduce_scatter x1, waiting for transfers between devices, on_device(): lax.psum_scatter((jnp.dot(mixed_wide, output_wide, preferred_element_type...  67.6 us
    all_gather x3, blocking collectives, carried_in(): lax.all_gather(a.astype(kind), axis)  60.1 us
    reduce_scatter x1, waiting for transfers between devices, on_device(): lax.psum_scatter(down_sum.astype(jnp.bfloat16), 'tp', scatter_dimension=0...  37.7 us
    all_gather x1, waiting for transfers between devices, on_device(): lax.all_gather(row_norm(middle, norm_gain), 'tp', axis=0, tiled=True)  27.7 us
    dynamic_update_slice x18, local copies, waits for them, and re-layouts, local_group(): lax.scan(block_step, carried, (query_rot.reshape(blocks, BLOCK, count_of_...  21.1 us
    unnamed x1, blocking collectives  16.7 us
  transfers between devices with their start and end apart: 5, of which 5 were waited for; matrix products, arithmetic and copies ran while one was open for 2% of the time, Pallas kernels for 0%

commit v1 on v0

--- a/solution.py
+++ b/solution.py
@@ -1,6 +1,10 @@
+import functools
 import jax
 import jax.numpy as jnp
+import numpy as np
 from jax import lax
+from jax.experimental import pallas as pl
+from jax.experimental.pallas import tpu as pltpu
 from jax.sharding import PartitionSpec as P
 
 HDW = 128
@@ -194,6 +198,442 @@
     return (middle.astype(jnp.float32) + down_rows).astype(jnp.bfloat16)
 
 
+F32 = jnp.float32
+BF16 = jnp.bfloat16
+MESH_ID = pl.DeviceIdType.MESH
+
+
+def turn_tables(shards, length):
+    lane = np.arange(128)
+    offsets, starts = [], []
+    for width in (HDW, HDN):
+        half = width // 2
+        inverse = rope_base ** (-((lane % half).astype(np.float64)) / half)
+        inside = np.arange(BLOCK)[:, None] * inverse[None, :]
+        first = (np.arange(shards * length // BLOCK) * BLOCK)[:, None] * inverse[None, :]
+        offsets += [np.cos(inside), np.sin(inside)]
+        starts += [np.cos(first), np.sin(first)]
+    return np.stack(offsets).astype(np.float32), np.stack(starts).astype(np.float32)
+
+
+def dot(a, b):
+    return jnp.dot(a, b, preferred_element_type=F32)
+
+
+def dot_rows(a, b):
+    return lax.dot_general(a, b, (((0,), (0,)), ((), ())), preferred_element_type=F32)
+
+
+def dot_cols(a, b):
+    return lax.dot_general(a, b, (((1,), (1,)), ((), ())), preferred_element_type=F32)
+
+
+def layer_kernel(
+    SP, TP,
+    stream, qw, kw, vw, gw, qn, kn, vn, gn, decay, offs, starts, gain, ow_w, ow_n, up, down,
+    out,
+    up_buf, down_buf, ow_buf, st_in, k_rot, before, inside, mixed, mix_in, mid, rows, hidden, part, part_in,
+    ssem, rsem, lsem,
+):
+    sp = lax.axis_index("sp")
+    tp = lax.axis_index("tp")
+    NZ = SP // 2
+    z = sp // 2
+    y = sp % 2
+    T = qw.shape[0]
+    NB = T // BLOCK
+    RT = T // TP
+    RB = up.shape[0]
+    CB = down.shape[1]
+    D = stream.shape[1]
+    FH = up.shape[1]
+    mate = tp + 1 - 2 * (tp % 2)
+
+    def at(dz, dy):
+        return ((z + dz) % NZ) * 2 + (y + dy) % 2
+
+    count = [0]
+    pending = []
+
+    def send(src, dst, device):
+        k = count[0]
+        count[0] += 1
+        copy = pltpu.make_async_remote_copy(
+            src_ref=src, dst_ref=dst, send_sem=ssem.at[k], recv_sem=rsem.at[k],
+            device_id=device, device_id_type=MESH_ID,
+        )
+        copy.start()
+        pending.append(copy)
+        return copy
+
+    def to_sp(i):
+        return (i, tp)
+
+    def to_tp(i):
+        return (sp, i)
+
+    barrier = pltpu.get_barrier_semaphore()
+    for d in range(1, SP):
+        pl.semaphore_signal(barrier, inc=1, device_id=to_sp((sp + d) % SP), device_id_type=MESH_ID)
+    for d in range(1, TP):
+        pl.semaphore_signal(barrier, inc=1, device_id=to_tp((tp + d) % TP), device_id_type=MESH_ID)
+    pl.semaphore_wait(barrier, SP + TP - 2)
+
+    def up_at(i, lo=0, n=RB):
+        return up_buf.at[pl.ds(pl.multiple_of(i * RB + lo, RB // 2), n), :]
+
+    def down_at(i, lo=0, n=FH):
+        return down_buf.at[i, pl.ds(lo, n), :]
+
+    above, below, across_y = to_sp(at(1, 0)), to_sp(at(-1, 0)), to_sp(at(0, 1))
+    a_y, a_p, a_m, b_y, b_p, c_p, c_m, d_m = ({} for _ in range(8))
+    place = {"up": up_at, "down": down_at}
+    own = {"up": up, "down": down}
+    full = {"up": RB, "down": FH}
+
+    def first_y(w):
+        a_y[w] = send(own[w], place[w](sp), across_y)
+
+    def first_p(w):
+        a_p[w] = send(own[w], place[w](sp), above)
+
+    def first_m(w):
+        a_m[w] = send(own[w], place[w](sp), below)
+
+    def second_y(w):
+        b_y[w] = send(place[w](at(1, 0)), place[w](at(1, 0)), across_y)
+
+    def second_p(w):
+        b_p[w] = send(place[w](at(0, 1)), place[w](at(0, 1)), above)
+
+    def half_p(w):
+        h = full[w] // 2
+        c_p[w] = send(place[w](at(-1, 0), 0, h), place[w](at(-1, 0), 0, h), above)
+
+    def half_m(w):
+        h = full[w] // 2
+        c_m[w] = send(place[w](at(1, 0), h, h), place[w](at(1, 0), h, h), below)
+
+    def third_m(w):
+        d_m[w] = send(place[w](at(1, 1)), place[w](at(1, 1)), below)
+
+    first_y("up")
+    first_p("up")
+    first_m("up")
+
+    locals_ = []
+
+    def keep(src, dst):
+        copy = pltpu.make_async_copy(src, dst, lsem.at[len(locals_)])
+        copy.start()
+        locals_.append(copy)
+
+    def ow_at(i, g):
+        return ow_buf.at[i, pl.ds(g * 128, 128), :]
+
+    ow_mate = [send(r, ow_at(tp, g), to_tp(mate)) for g, r in enumerate((ow_w, ow_n))]
+    ow_far = [
+        (q, g, send(r, ow_at(tp, g), to_tp((tp + 2 * q) % TP)))
+        for q in range(1, TP // 2) for g, r in enumerate((ow_w, ow_n))
+    ]
+    keep(up, up_at(sp))
+    keep(down, down_at(sp))
+    keep(ow_w, ow_at(tp, 0))
+    keep(ow_n, ow_at(tp, 1))
+
+    lane = lax.broadcasted_iota(jnp.int32, (128, 128), 1)
+    row = lax.broadcasted_iota(jnp.int32, (128, 128), 0)
+    lower = row >= lane
+    low = lane < HDN
+    low_row = row < HDN
+    diagonal = low == low_row
+    cr = decay[...]
+    step = 1
+    while step < 128:
+        cr = cr + jnp.where(lane >= step, pltpu.roll(cr, step, 1), 0.0)
+        step *= 2
+    ct = cr.T
+
+    def col(h, b):
+        return ct[:, h * NB + b:h * NB + b + 1]
+
+    def line(h, b):
+        return cr[h * NB + b:h * NB + b + 1, :]
+
+    def total(h, b):
+        return cr[h * NB + b:h * NB + b + 1, 127:128]
+
+    def pair(a, b):
+        return jnp.where(low, a, b)
+
+    sign_w = jnp.where(low, -1.0, 1.0)
+    early = (lane % HDN) < HDN // 2
+    sign_n = jnp.where(early, -1.0, 1.0)
+
+    def tables(g, b):
+        cb = starts[2 * g, pl.ds(sp * NB + b, 1), :]
+        sb = starts[2 * g + 1, pl.ds(sp * NB + b, 1), :]
+        co, so = offs[2 * g], offs[2 * g + 1]
+        return co * cb - so * sb, (so * cb + co * sb) * (sign_n if g else sign_w)
+
+    def turned(x, table, g):
+        if g:
+            other = jnp.where(early, pltpu.roll(x, 128 - HDN // 2, 1), pltpu.roll(x, HDN // 2, 1))
+        else:
+            other = pltpu.roll(x, HDW // 2, 1)
+        return x * table[0] + other * table[1]
+
+    state_w = jnp.zeros((128, 128), F32)
+    state_n = jnp.zeros((128, 128), F32)
+    sums = [jnp.zeros((1, 1), F32) for _ in range(3)]
+    for b in range(NB):
+        rs = pl.ds(b * BLOCK, BLOCK)
+        before[0, b] = state_w
+        before[1, b] = state_n
+        kwr = turned(kw[rs, :].astype(F32), tables(0, b), 0) * HDW ** (-0.5)
+        knr = turned(kn[rs, :].astype(F32), tables(1, b), 1) * HDN ** (-0.5)
+        k_rot[rs, 0:128] = kwr.astype(BF16)
+        k_rot[rs, 128:256] = knr.astype(BF16)
+        t0, t1, t2 = total(0, b), total(1, b), total(2, b)
+        sums = [s + t for s, t in zip(sums, (t0, t1, t2))]
+        tail_w = jnp.exp(t0 - col(0, b))
+        tail_n = pair(jnp.exp(t1 - col(1, b)), jnp.exp(t2 - col(2, b)))
+        state_w = jnp.exp(t0) * state_w + dot_rows((kwr * tail_w).astype(BF16), vw[rs, :])
+        grown = dot_rows((knr * tail_n).astype(BF16), vn[rs, :])
+        state_n = jnp.where(low_row, jnp.exp(t1), jnp.exp(t2)) * state_n + jnp.where(diagonal, grown, 0.0)
+    small = lax.broadcasted_iota(jnp.int32, (16, 128), 0)
+    rates = jnp.where(small == 0, jnp.exp(sums[0]), jnp.where(small == 1, jnp.exp(sums[1]), jnp.exp(sums[2])))
+    st_in[sp, 0:128, :] = state_w.astype(BF16)
+    st_in[sp, 128:256, :] = state_n.astype(BF16)
+    st_in[sp, 256:272, :] = rates.astype(BF16)
+    states = [send(st_in.at[sp], st_in.at[sp], to_sp((sp + d) % SP)) for d in range(1, SP)]
+
+    for b in range(NB):
+        rs = pl.ds(b * BLOCK, BLOCK)
+        kwr, knr = k_rot[rs, 0:128], k_rot[rs, 128:256]
+        qwr = turned(qw[rs, :].astype(F32), tables(0, b), 0)
+        qnr = turned(qn[rs, :].astype(F32), tables(1, b), 1)
+
+        def factor(h):
+            return jnp.where(lower, jnp.exp(jnp.minimum(col(h, b) - line(h, b), 0.0)), 0.0)
+
+        scores = (dot_cols(qwr.astype(BF16), kwr) * factor(0)).astype(BF16)
+        inside[rs, 0:128] = dot(scores, vw[rs, :])
+        near = (dot_cols(jnp.where(low, qnr, 0.0).astype(BF16), knr) * factor(1)).astype(BF16)
+        far = (dot_cols(jnp.where(low, 0.0, qnr).astype(BF16), knr) * factor(2)).astype(BF16)
+        inside[rs, 128:256] = pair(dot(near, vn[rs, :]), dot(far, vn[rs, :]))
+        k_rot[rs, 0:128] = (qwr * jnp.exp(col(0, b))).astype(BF16)
+        k_rot[rs, 128:256] = (qnr * pair(jnp.exp(col(1, b)), jnp.exp(col(2, b)))).astype(BF16)
+
+    a_y["up"].wait_recv()
+    a_p["up"].wait_recv()
+    a_m["up"].wait_recv()
+    second_y("up")
+    first_y("down")
+    second_p("up")
+    half_p("up")
+    first_p("down")
+    half_m("up")
+    first_m("down")
+
+    for copy in states:
+        copy.wait_recv()
+    s_w = jnp.zeros((128, 128), F32)
+    s_n = jnp.zeros((128, 128), F32)
+    for j in range(SP):
+        r = st_in[j, 256:272, :].astype(F32)
+        s_w = jnp.where(j < sp, s_w * r[0:1, :] + st_in[j, 0:128, :].astype(F32), s_w)
+        s_n = jnp.where(
+            j < sp, s_n * jnp.where(low_row, r[1:2, :], r[2:3, :]) + st_in[j, 128:256, :].astype(F32), s_n
+        )
+
+    sums = [jnp.zeros((1, 1), F32) for _ in range(3)]
+    for b in range(NB):
+        rs = pl.ds(b * BLOCK, BLOCK)
+        whole_w = before[0, b] + jnp.exp(sums[0]) * s_w
+        whole_n = before[1, b] + jnp.where(low_row, jnp.exp(sums[1]), jnp.exp(sums[2])) * s_n
+        sums = [s + total(h, b) for h, s in enumerate(sums)]
+        o_w = inside[rs, 0:128] + dot(k_rot[rs, 0:128], whole_w.astype(BF16))
+        o_n = inside[rs, 128:256] + dot(k_rot[rs, 128:256], whole_n.astype(BF16))
+
+        def both(x):
+            first = jnp.sum(jnp.where(low, x, 0.0), axis=-1, keepdims=True) / HDN
+            second = jnp.sum(jnp.where(low, 0.0, x), axis=-1, keepdims=True) / HDN
+            return pair(first, second)
+
+        c_w = o_w - jnp.mean(o_w, axis=-1, keepdims=True)
+        n_w = c_w * lax.rsqrt(jnp.mean(c_w * c_w, axis=-1, keepdims=True) + head_eps)
+        c_n = o_n - both(o_n)
+        n_n = c_n * lax.rsqrt(both(c_n * c_n) + head_eps)
+        mixed[rs, 0:128] = (jax.nn.silu(gw[rs, :].astype(F32)) * n_w).astype(BF16)
+        mixed[rs, 128:256] = (jax.nn.silu(gn[rs, :].astype(F32)) * n_n).astype(BF16)
+
+    def my_rows(i):
+        return pl.ds(pl.multiple_of(i * RT, RT), RT)
+
+    swaps = [
+        send(mixed.at[my_rows((tp + d) % TP), :], mix_in.at[tp], to_tp((tp + d) % TP)) for d in range(1, TP)
+    ]
+    mix_in[tp] = mixed[my_rows(tp), :]
+    ow_relay = []
+    for q, g, copy in ow_far:
+        copy.wait_recv()
+        came = (tp + TP - 2 * q) % TP
+        ow_relay.append(send(ow_at(came, g), ow_at(came, g), to_tp(mate)))
+    b_y["up"].wait_recv()
+    third_m("up")
+    for copy in swaps + ow_mate + ow_relay:
+        copy.wait_recv()
+    for copy in locals_:
+        copy.wait()
+
+    def project(c, _):
+        cs = pl.ds(pl.multiple_of(c * 512, 512), 512)
+        acc = stream[:, cs].astype(F32)
+        for i in range(TP):
+            acc = acc + dot(mix_in[i], ow_buf[i, :, cs])
+        mid[:, cs] = acc.astype(BF16)
+        return 0
+
+    lax.fori_loop(0, D // 512, project, 0)
+
+    def norm(i, _):
+        m = mid[pl.ds(pl.multiple_of(i * 32, 32), 32), :].astype(F32)
+        scale = lax.rsqrt(jnp.mean(m * m, axis=-1, keepdims=True) + norm_eps)
+        rows[pl.ds(pl.multiple_of(tp * RT + i * 32, 32), 32), :] = (m * scale * gain[...].astype(F32)).astype(BF16)
+        return 0
+
+    lax.fori_loop(0, RT // 32, norm, 0)
+    mine = rows.at[my_rows(tp), :]
+    row_far = [(q, send(mine, mine, to_tp((tp + 2 * q) % TP))) for q in range(1, TP // 2)]
+    row_mate = send(mine, mine, to_tp(mate))
+
+    a_m["down"].wait_recv()
+    second_y("down")
+    half_m("down")
+    row_relay = []
+    for q, copy in row_far:
+        copy.wait_recv()
+        came = rows.at[my_rows((tp + TP - 2 * q) % TP), :]
+        row_relay.append((q, send(came, came, to_tp(mate))))
+    a_y["down"].wait_recv()
+    second_p("down")
+    for c in (b_p, c_p, c_m, d_m):
+        c["up"].wait_recv()
+    a_p["down"].wait_recv()
+    half_p("down")
+    row_mate.wait_recv()
+
+    def up_rows(i):
+        rs = pl.ds(pl.multiple_of(i * 2 * RT, 2 * RT), 2 * RT)
+
+        def one(c, _):
+            cs = pl.ds(pl.multiple_of(c * 512, 512), 512)
+            h = jnp.maximum(dot(rows[rs, :], up_buf[:, cs]), 0.0)
+            hidden[rs, cs] = (h * h).astype(BF16)
+            return 0
+
+        lax.fori_loop(0, FH // 512, one, 0)
+
+    up_rows(tp // 2)
+    for q, copy in row_relay:
+        copy.wait_recv()
+        up_rows(((tp + TP - 2 * q) % TP) // 2)
+
+    def chunk(k, j):
+        def one(i, _):
+            rs = pl.ds(pl.multiple_of(i * 2 * RT, 2 * RT), 2 * RT)
+            part[k, rs, :] = dot(hidden[rs, :], down_buf[j]).astype(BF16)
+            return 0
+
+        lax.fori_loop(0, TP // 2, one, 0)
+        return [
+            send(part.at[k, my_rows((tp + d) % TP), :], part_in.at[k, d - 1], to_tp((tp + d) % TP))
+            for d in range(1, TP)
+        ]
+
+    def finish(k, j, copies):
+        for copy in copies:
+            copy.wait_recv()
+        cs = pl.ds(pl.multiple_of(j * CB, CB), CB)
+        acc = mid[:, cs].astype(F32) + part[k, my_rows(tp), :].astype(F32)
+        for d in range(TP - 1):
+            acc = acc + part_in[k, d].astype(F32)
+        out[:, cs] = acc.astype(BF16)
+
+    order = [
+        (at(0, 0), []), (at(1, 0), []), (at(0, 1), []), (at(-1, 0), []),
+        (at(1, 1), [b_y]), (at(2, 0), [c_p, c_m]), (at(-1, 1), [b_p]), (at(2, 1), [d_m]),
+    ]
+    done = []
+    for k, (j, needs) in enumerate(order):
+        for c in needs:
+            c["down"].wait_recv()
+            if c is b_y:
+                third_m("down")
+        done.append((k, j, chunk(k, j)))
+        if k:
+            finish(*done[k - 1])
+    finish(*done[-1])
+    for copy in pending:
+        copy.wait_send()
+
+
+def one_kernel(SP, TP, *args):
+    (stream, qw, kw, vw, gw, dw, qn, kn, vn, gn, dn, ow, on, gain, up, down) = args
+    T = qw.shape[0]
+    NB = T // BLOCK
+    D = stream.shape[1]
+    RT = T // TP
+    FH = up.shape[1]
+    CB = down.shape[1]
+    heads = dw.shape[0] + dn.shape[0]
+    decay = jnp.concatenate([dw, dn]).reshape(heads * NB, BLOCK)
+    decay = jnp.pad(decay, ((0, 128 - heads * NB), (0, 0)))
+    offs, starts = turn_tables(SP, T)
+    vmem = pl.BlockSpec(memory_space=pltpu.VMEM)
+    hbm = pl.BlockSpec(memory_space=pl.ANY)
+    copies = 72
+    return pl.pallas_call(
+        functools.partial(layer_kernel, SP, TP),
+        out_shape=jax.ShapeDtypeStruct((RT, D), BF16),
+        in_specs=[vmem] * 13 + [hbm] * 4,
+        out_specs=vmem,
+        scratch_shapes=[
+            pltpu.VMEM((D, FH), BF16),
+            pltpu.VMEM((SP, FH, CB), BF16),
+            pltpu.VMEM((TP, 256, D), BF16),
+            pltpu.VMEM((SP, 272, 128), BF16),
+            pltpu.VMEM((T, 256), BF16),
+            pltpu.VMEM((2, NB, 128, 128), F32),
+            pltpu.VMEM((T, 256), F32),
+            pltpu.VMEM((T, 256), BF16),
+            pltpu.VMEM((TP, RT, 256), BF16),
+            pltpu.VMEM((RT, D), BF16),
+            pltpu.VMEM((T, D), BF16),
+            pltpu.VMEM((T, FH), BF16),
+            pltpu.VMEM((SP, T, CB), BF16),
+            pltpu.VMEM((SP, TP - 1, RT, CB), BF16),
+            pltpu.SemaphoreType.DMA((copies,)),
+            pltpu.SemaphoreType.DMA((copies,)),
+            pltpu.SemaphoreType.DMA((4,)),
+        ],
+        compiler_params=pltpu.CompilerParams(
+            collective_id=0, has_side_effects=True, vmem_limit_bytes=60 * 1024 * 1024
+        ),
+    )(stream, qw, kw, vw, gw, qn, kn, vn, gn, decay, jnp.asarray(offs), jnp.asarray(starts),
+      gain.reshape(1, D), ow, on, up, down)
+
+
+def fits_kernel(SP, TP, args):
+    D, FF = args[14].shape
+    T = args[1].shape[0] // SP
+    return (
+        SP == 8 and TP == 4 and D % (SP * 128) == 0 and T % (TP * 32) == 0 and T % BLOCK == 0
+        and args[1].shape[1] == TP * 128 and args[6].shape[1] == TP * 128
+    )
+
+
 def solution(mesh):
     in_specs = (
         P(("sp", "tp"), None),
@@ -214,6 +654,12 @@
         P("tp", "sp"),
     )
     out_specs = P(("sp", "tp"), None)
-    return jax.shard_map(
-        on_device, mesh=mesh, in_specs=in_specs, out_specs=out_specs, check_vma=False
-    )
+    SP, TP = mesh.shape["sp"], mesh.shape["tp"]
+
+    def layer(*args):
+        body = functools.partial(one_kernel, SP, TP) if fits_kernel(SP, TP, args) else on_device
+        return jax.shard_map(
+            body, mesh=mesh, in_specs=in_specs, out_specs=out_specs, check_vma=False
+        )(*args)
+
+    return layer

time: 580 us -> 265 us (0.46)
  waiting for transfers between devices: 372 us -> 0 us
  Pallas kernels: 0 us -> 261 us
  blocking collectives: 76.8 us -> 0 us
  local copies, waits for them, and re-layouts: 42.9 us -> 4.06 us
  matrix products: 36.5 us -> 0 us
  other arithmetic: 25.9 us -> 0.01 us
  between operations: 14.9 us -> 0.02 us
  loops' own time: 7.6 us -> 0 us
    all_gather x3 -> x0, waiting for transfers between devices: 266 us -> none  [the longest x1 125 us: on_device(): lax.all_gather(up_weight, 'sp', axis=0, tiled=True)]
    pallas_call x0 -> x1, Pallas kernels: none -> 261 us  [one_kernel(): pl.pallas_call(functools.partial(layer_kernel, SP, TP), out_shape=jax.Sha...]
    reduce_scatter x2 -> x0, waiting for transfers between devices: 105 us -> none  [the longest x1 67.6 us: on_device(): lax.psum_scatter((jnp.dot(mixed_wide, output_wide, preferred_element_type...]
    all_gather x3 -> x0, blocking collectives: 60.1 us -> none  [carried_in(): lax.all_gather(a.astype(kind), axis)]
    dot_general x42 -> x0, matrix products: 36.5 us -> none  [the longest x1 11.9 us: on_device(): jnp.dot(hidden, lax.all_gather(down_weight, 'sp', axis=1, tiled=True), pr...]
    dynamic_update_slice x18 -> x0, local copies, waits for them, and re-layouts: 21.1 us -> none  [local_group(): lax.scan(block_step, carried, (query_rot.reshape(blocks, BLOCK, count_of_...]
    unnamed x1 -> x0, blocking collectives: 16.7 us -> none
    another operation x3 -> x0, loops' own time: 7.6 us -> none  [the longest x2 4.94 us: local_group(): lax.scan(block_step, carried, (query_rot.reshape(blocks, BLOCK, count_of_...]
  transfers between devices with their start and end apart: 5 -> 0, of which waited for: 5 -> 0; matrix products, arithmetic and copies ran while one was open for 2% -> 0% of each run, Pallas kernels for 0% -> 0%
where the time goes in v1:
time: 265 us
  Pallas kernels  261 us (98%)
  local copies, waits for them, and re-layouts  4.06 us (2%)
    pallas_call x1, Pallas kernels, one_kernel(): pl.pallas_call(functools.partial(layer_kernel, SP, TP), out_shape=jax.Sha...  261 us

profile of v1, /device:TPU:17, one launch (start us, length us, event | category | flops | bytes accessed | tf_op | source)
XLA Modules:
  0.0 264.7 jit_solution(2663715856609502908)
XLA Ops:
  0.0 0.0 copy-start
  0.0 0.0 copy-start.1
  0.0 1.3 reshape.7.gain
  1.3 0.0 copy-done
  1.3 0.0 copy-done.1
  1.4 0.6 pad.4.decay
  2.0 260.6 %shard_map.172 = bf16[192,2048]{1,0:T(8,128)(2,1)} custom-call(bf16[192,2048]{1,0:T(8,128)(2,1)} %stream.1, bf16[768,128]{1,0:T(8,128)(2,1)} %qw.1, bf16[768,128]{1,0:T(8,128)(2,1)} %kw.1, bf16[768,128]{1,0:T(8,128)(2,1)} %vw.1, bf16[768,128]{1,0:T(8,128)(2,1)} %gw.1, bf16[768,128]{1,0:T(8,128)(2,1)} %qn.1, bf16[768,128]{1,0:T(8,128)(2,1)} %kn.1, ...), custom_call_target="tpu_custom_call" | custom-call | tf_op jit(solution)/shard_map/pallas_call | solution.py:597
  262.6 2.1 copy.20
  (2 shorter events, 0.0 us)
Async XLA Ops:
  0.0 1.3 copy-start
  0.0 1.3 copy-start.1

commit v2 on v1

--- a/solution.py
+++ b/solution.py
@@ -233,7 +233,7 @@
     stream, qw, kw, vw, gw, qn, kn, vn, gn, decay, offs, starts, gain, ow_w, ow_n, up, down,
     out,
     up_buf, down_buf, ow_buf, st_in, k_rot, before, inside, mixed, mix_in, mid, rows, hidden, part, part_in,
-    ssem, rsem, lsem,
+    ssem, rsem, lsem, zsend, zrecv,
 ):
     sp = lax.axis_index("sp")
     tp = lax.axis_index("tp")
@@ -246,7 +246,7 @@
     RB = up.shape[0]
     CB = down.shape[1]
     D = stream.shape[1]
-    FH = up.shape[1]
+    FH = up.shape[1] // 2
     mate = tp + 1 - 2 * (tp % 2)
 
     def at(dz, dy):
@@ -266,6 +266,9 @@
         pending.append(copy)
         return copy
 
+    def group(dy, dt):
+        return (z * 2 + (y + dy) % 2, (tp + dt) % TP)
+
     def to_sp(i):
         return (i, tp)
 
@@ -277,49 +280,72 @@
         pl.semaphore_signal(barrier, inc=1, device_id=to_sp((sp + d) % SP), device_id_type=MESH_ID)
     for d in range(1, TP):
         pl.semaphore_signal(barrier, inc=1, device_id=to_tp((tp + d) % TP), device_id_type=MESH_ID)
-    pl.semaphore_wait(barrier, SP + TP - 2)
-
-    def up_at(i, lo=0, n=RB):
-        return up_buf.at[pl.ds(pl.multiple_of(i * RB + lo, RB // 2), n), :]
-
-    def down_at(i, lo=0, n=FH):
-        return down_buf.at[i, pl.ds(lo, n), :]
-
-    above, below, across_y = to_sp(at(1, 0)), to_sp(at(-1, 0)), to_sp(at(0, 1))
-    a_y, a_p, a_m, b_y, b_p, c_p, c_m, d_m = ({} for _ in range(8))
-    place = {"up": up_at, "down": down_at}
-    own = {"up": up, "down": down}
-    full = {"up": RB, "down": FH}
-
-    def first_y(w):
-        a_y[w] = send(own[w], place[w](sp), across_y)
-
-    def first_p(w):
-        a_p[w] = send(own[w], place[w](sp), above)
-
-    def first_m(w):
-        a_m[w] = send(own[w], place[w](sp), below)
-
-    def second_y(w):
-        b_y[w] = send(place[w](at(1, 0)), place[w](at(1, 0)), across_y)
-
-    def second_p(w):
-        b_p[w] = send(place[w](at(0, 1)), place[w](at(0, 1)), above)
-
-    def half_p(w):
-        h = full[w] // 2
-        c_p[w] = send(place[w](at(-1, 0), 0, h), place[w](at(-1, 0), 0, h), above)
-
-    def half_m(w):
-        h = full[w] // 2
-        c_m[w] = send(place[w](at(1, 0), h, h), place[w](at(1, 0), h, h), below)
-
-    def third_m(w):
-        d_m[w] = send(place[w](at(1, 1)), place[w](at(1, 1)), below)
-
-    first_y("up")
-    first_p("up")
-    first_m("up")
+    for d in range(1, TP):
+        pl.semaphore_signal(barrier, inc=1, device_id=group(1, d), device_id_type=MESH_ID)
+    pl.semaphore_wait(barrier, SP + 2 * TP - 3)
+
+    def up_at(i):
+        return up_buf.at[pl.ds(pl.multiple_of(i * RB, RB), RB), :]
+
+    def down_at(i):
+        return down_buf.at[i]
+
+    place = (up_at, down_at)
+
+    def hidden_half(w, half):
+        cut = pl.ds(pl.multiple_of(half * FH, FH), FH)
+        return up.at[:, cut] if w == 0 else down.at[cut, :]
+
+    across_y = to_sp(at(0, 1))
+    line_waits = []
+
+    def piece(w, dy, zs):
+        return place[w](zs * 2 + (y + dy) % 2)
+
+    def line_copy(w, dy, zs, src, slot, device_z):
+        return pltpu.make_async_remote_copy(
+            src_ref=src, dst_ref=piece(w, dy, zs), send_sem=zsend.at[slot],
+            recv_sem=zrecv.at[(w * 2 + dy) * NZ + zs],
+            device_id=to_sp(device_z * 2 + y), device_id_type=MESH_ID,
+        )
+
+    def line_start(when, copy):
+        @pl.when(when)
+        def _():
+            copy.start()
+
+        line_waits.append((when, copy))
+
+    def line_send(w, dy):
+        for t in (1, 2, 0, 3):
+            src = hidden_half(w, y) if dy == 0 else piece(w, dy, z)
+            far = ((z == 0) & (t == 3)) | ((z == NZ - 1) & (t == 0))
+            line_start((z != t) & jnp.logical_not(far), line_copy(w, dy, z, src, (w * 2 + dy) * 5 + t, t))
+
+    def line_wait(w, dy, zs):
+        line_copy(w, dy, zs, piece(w, dy, zs), 0, (z + 1) % NZ).wait_recv()
+
+    def line_relay(w, dy):
+        for me, source, target in ((2, 0, 3), (1, 3, 0)):
+            @pl.when(z == me)
+            def _():
+                line_wait(w, dy, source)
+
+            slot = (w * 2 + dy) * 5 + 4
+            line_start(z == me, line_copy(w, dy, source, piece(w, dy, source), slot, target))
+
+    def line_arrived(w, dy, d):
+        zs = (z + d * (1 + 2 * (z // 2))) % NZ
+        relayed = ((z == 2) & (zs == 0)) | ((z == 1) & (zs == 3))
+
+        @pl.when(jnp.logical_not(relayed))
+        def _():
+            line_wait(w, dy, zs)
+
+        return zs * 2 + (y + dy) % 2
+
+    up_y = send(hidden_half(0, (y + 1) % 2), up_at(sp), across_y)
+    line_send(0, 0)
 
     locals_ = []
 
@@ -336,8 +362,8 @@
         (q, g, send(r, ow_at(tp, g), to_tp((tp + 2 * q) % TP)))
         for q in range(1, TP // 2) for g, r in enumerate((ow_w, ow_n))
     ]
-    keep(up, up_at(sp))
-    keep(down, down_at(sp))
+    keep(hidden_half(0, y), up_at(sp))
+    keep(hidden_half(1, y), down_at(sp))
     keep(ow_w, ow_at(tp, 0))
     keep(ow_n, ow_at(tp, 1))
 
@@ -425,16 +451,10 @@
         k_rot[rs, 0:128] = (qwr * jnp.exp(col(0, b))).astype(BF16)
         k_rot[rs, 128:256] = (qnr * pair(jnp.exp(col(1, b)), jnp.exp(col(2, b)))).astype(BF16)
 
-    a_y["up"].wait_recv()
-    a_p["up"].wait_recv()
-    a_m["up"].wait_recv()
-    second_y("up")
-    first_y("down")
-    second_p("up")
-    half_p("up")
-    first_p("down")
-    half_m("up")
-    first_m("down")
+    up_y.wait_recv()
+    line_send(0, 1)
+    down_y = send(hidden_half(1, (y + 1) % 2), down_at(sp), across_y)
+    line_send(1, 0)
 
     for copy in states:
         copy.wait_recv()
@@ -480,8 +500,7 @@
         copy.wait_recv()
         came = (tp + TP - 2 * q) % TP
         ow_relay.append(send(ow_at(came, g), ow_at(came, g), to_tp(mate)))
-    b_y["up"].wait_recv()
-    third_m("up")
+    line_relay(0, 0)
     for copy in swaps + ow_mate + ow_relay:
         copy.wait_recv()
     for copy in locals_:
@@ -500,31 +519,31 @@
     def norm(i, _):
         m = mid[pl.ds(pl.multiple_of(i * 32, 32), 32), :].astype(F32)
         scale = lax.rsqrt(jnp.mean(m * m, axis=-1, keepdims=True) + norm_eps)
-        rows[pl.ds(pl.multiple_of(tp * RT + i * 32, 32), 32), :] = (m * scale * gain[...].astype(F32)).astype(BF16)
+        rows[pl.ds(pl.multiple_of((y * TP + tp) * RT + i * 32, 32), 32), :] = (m * scale * gain[...].astype(F32)).astype(BF16)
         return 0
 
     lax.fori_loop(0, RT // 32, norm, 0)
-    mine = rows.at[my_rows(tp), :]
-    row_far = [(q, send(mine, mine, to_tp((tp + 2 * q) % TP))) for q in range(1, TP // 2)]
-    row_mate = send(mine, mine, to_tp(mate))
-
-    a_m["down"].wait_recv()
-    second_y("down")
-    half_m("down")
-    row_relay = []
-    for q, copy in row_far:
-        copy.wait_recv()
-        came = rows.at[my_rows((tp + TP - 2 * q) % TP), :]
-        row_relay.append((q, send(came, came, to_tp(mate))))
-    a_y["down"].wait_recv()
-    second_p("down")
-    for c in (b_p, c_p, c_m, d_m):
-        c["up"].wait_recv()
-    a_p["down"].wait_recv()
-    half_p("down")
-    row_mate.wait_recv()
-
-    def up_rows(i):
+
+    def block(dy, dt):
+        return rows.at[my_rows((y + dy) % 2 * TP + (tp + dt) % TP), :]
+
+    near_x = send(block(0, 0), block(0, 0), group(0, 2))
+    near_y = send(block(0, 0), block(0, 0), group(1, 0))
+    hand = [send(block(0, 0), block(0, 0), to_tp(mate))]
+    line_relay(0, 1)
+    down_y.wait_recv()
+    line_send(1, 1)
+    near_x.wait_recv()
+    corner = send(block(0, 2), block(0, 2), group(1, 0))
+    hand.append(send(block(0, 2), block(0, 2), to_tp(mate)))
+    near_y.wait_recv()
+    hand.append(send(block(1, 0), block(1, 0), to_tp(mate)))
+    for dy in range(2):
+        for d in range(1, NZ):
+            line_arrived(0, dy, d)
+
+    def up_rows(dy, dp):
+        i = (y + dy) % 2 * (TP // 2) + (tp // 2 + dp) % (TP // 2)
         rs = pl.ds(pl.multiple_of(i * 2 * RT, 2 * RT), 2 * RT)
 
         def one(c, _):
@@ -535,10 +554,19 @@
 
         lax.fori_loop(0, FH // 512, one, 0)
 
-    up_rows(tp // 2)
-    for q, copy in row_relay:
-        copy.wait_recv()
-        up_rows(((tp + TP - 2 * q) % TP) // 2)
+    hand[0].wait_recv()
+    up_rows(0, 0)
+    corner.wait_recv()
+    hand.append(send(block(1, 2), block(1, 2), to_tp(mate)))
+    line_relay(1, 0)
+    hand[1].wait_recv()
+    up_rows(0, 1)
+    hand[2].wait_recv()
+    up_rows(1, 0)
+    hand[3].wait_recv()
+    up_rows(1, 1)
+
+    peers = [(dy, dt) for dy in range(2) for dt in range(TP) if dy or dt]
 
     def chunk(k, j):
         def one(i, _):
@@ -546,35 +574,39 @@
             part[k, rs, :] = dot(hidden[rs, :], down_buf[j]).astype(BF16)
             return 0
 
-        lax.fori_loop(0, TP // 2, one, 0)
+        lax.fori_loop(0, TP, one, 0)
         return [
-            send(part.at[k, my_rows((tp + d) % TP), :], part_in.at[k, d - 1], to_tp((tp + d) % TP))
-            for d in range(1, TP)
+            send(
+                part.at[k, my_rows((y + dy) % 2 * TP + (tp + dt) % TP), :],
+                part_in.at[k, dy * TP + dt - 1], group(dy, dt),
+            )
+            for dy, dt in peers
         ]
 
     def finish(k, j, copies):
         for copy in copies:
             copy.wait_recv()
         cs = pl.ds(pl.multiple_of(j * CB, CB), CB)
-        acc = mid[:, cs].astype(F32) + part[k, my_rows(tp), :].astype(F32)
-        for d in range(TP - 1):
+        acc = mid[:, cs].astype(F32) + part[k, my_rows(y * TP + tp), :].astype(F32)
+        for d in range(2 * TP - 1):
             acc = acc + part_in[k, d].astype(F32)
         out[:, cs] = acc.astype(BF16)
 
-    order = [
-        (at(0, 0), []), (at(1, 0), []), (at(0, 1), []), (at(-1, 0), []),
-        (at(1, 1), [b_y]), (at(2, 0), [c_p, c_m]), (at(-1, 1), [b_p]), (at(2, 1), [d_m]),
-    ]
     done = []
-    for k, (j, needs) in enumerate(order):
-        for c in needs:
-            c["down"].wait_recv()
-            if c is b_y:
-                third_m("down")
+    for k in range(SP):
+        d, dy = k // 2, (y + k) % 2
+        if k == 4:
+            line_relay(1, 1)
+        j = line_arrived(1, dy, d) if d else at(0, dy)
         done.append((k, j, chunk(k, j)))
-        if k:
-            finish(*done[k - 1])
+        if k > 1:
+            finish(*done[k - 2])
+    finish(*done[-2])
     finish(*done[-1])
+    for when, copy in line_waits:
+        @pl.when(when)
+        def _(copy=copy):
+            copy.wait_send()
     for copy in pending:
         copy.wait_send()
 
@@ -585,7 +617,7 @@
     NB = T // BLOCK
     D = stream.shape[1]
     RT = T // TP
-    FH = up.shape[1]
+    FH = up.shape[1] // 2
     CB = down.shape[1]
     heads = dw.shape[0] + dn.shape[0]
     decay = jnp.concatenate([dw, dn]).reshape(heads * NB, BLOCK)
@@ -593,7 +625,7 @@
     offs, starts = turn_tables(SP, T)
     vmem = pl.BlockSpec(memory_space=pltpu.VMEM)
     hbm = pl.BlockSpec(memory_space=pl.ANY)
-    copies = 72
+    copies = 96
     return pl.pallas_call(
         functools.partial(layer_kernel, SP, TP),
         out_shape=jax.ShapeDtypeStruct((RT, D), BF16),
@@ -610,13 +642,15 @@
             pltpu.VMEM((T, 256), BF16),
             pltpu.VMEM((TP, RT, 256), BF16),
             pltpu.VMEM((RT, D), BF16),
-            pltpu.VMEM((T, D), BF16),
-            pltpu.VMEM((T, FH), BF16),
-            pltpu.VMEM((SP, T, CB), BF16),
-            pltpu.VMEM((SP, TP - 1, RT, CB), BF16),
+            pltpu.VMEM((2 * T, D), BF16),
+            pltpu.VMEM((2 * T, FH), BF16),
+            pltpu.VMEM((SP, 2 * T, CB), BF16),
+            pltpu.VMEM((SP, 2 * TP - 1, RT, CB), BF16),
             pltpu.SemaphoreType.DMA((copies,)),
             pltpu.SemaphoreType.DMA((copies,)),
             pltpu.SemaphoreType.DMA((4,)),
+            pltpu.SemaphoreType.DMA((20,)),
+            pltpu.SemaphoreType.DMA((2 * SP,)),
         ],
         compiler_params=pltpu.CompilerParams(
             collective_id=0, has_side_effects=True, vmem_limit_bytes=60 * 1024 * 1024

time: 265 us -> 207 us (0.78); the launches traced: 265 us -> 203 us
  Pallas kernels: 261 us -> 199 us
    pallas_call x1, Pallas kernels: 261 us -> 199 us  [one_kernel(): pl.pallas_call(functools.partial(layer_kernel, SP, TP), out_shape=jax.Sha...]
where the time goes in v2:
time: 207 us; the launch traced here: 203 us
  Pallas kernels  199 us (96%)
  local copies, waits for them, and re-layouts  4.06 us (2%)
    pallas_call x1, Pallas kernels, one_kernel(): pl.pallas_call(functools.partial(layer_kernel, SP, TP), out_shape=jax.Sha...  199 us

profile of v2, /device:TPU:17, one launch (start us, length us, event | category | flops | bytes accessed | tf_op | source)
XLA Modules:
  0.0 202.9 jit_solution(6783226986436012211)
XLA Ops:
  0.0 0.0 copy-start
  0.0 0.0 copy-start.1
  0.0 1.3 reshape.7.gain
  1.3 0.0 copy-done
  1.3 0.0 copy-done.1
  1.4 0.6 pad.4.decay
  2.0 198.8 %shard_map.172 = bf16[192,2048]{1,0:T(8,128)(2,1)} custom-call(bf16[192,2048]{1,0:T(8,128)(2,1)} %stream.1, bf16[768,128]{1,0:T(8,128)(2,1)} %qw.1, bf16[768,128]{1,0:T(8,128)(2,1)} %kw.1, bf16[768,128]{1,0:T(8,128)(2,1)} %vw.1, bf16[768,128]{1,0:T(8,128)(2,1)} %gw.1, bf16[768,128]{1,0:T(8,128)(2,1)} %qn.1, bf16[768,128]{1,0:T(8,128)(2,1)} %kn.1, ...), custom_call_target="tpu_custom_call" | custom-call | tf_op jit(solution)/shard_map/pallas_call | solution.py:629
  200.8 2.1 %copy.20 = bf16[192,2048]{1,0:T(8,128)(2,1)} copy(bf16[192,2048]{1,0:T(8,128)(2,1)} %shard_map.172) | data formatting | bytes 1572864
  (2 shorter events, 0.0 us)
Async XLA Ops:
  0.0 1.3 copy-start
  0.0 1.3 copy-start.1
